TPU v7x, 32 devices: a whole 2x2x4 slice. The times are simulated.
32 devices in a mesh: sp: 8 (over z, x), tp: 4 (over y, core).
Axes of the slice: x: 2, y: 2, z: 4, core: 2. Of those that a mesh axis runs over, the one named last changes fastest.
Arguments:
- resid: bfloat16 [1024, 2048], P('sp'), may hold values from -6 to 6
- norm_gain: float32 [2048], replicated, may hold values from 0.1 to 1.9
- cotangent: bfloat16 [1024, 2048], P('sp'), may hold values from -6 to 6
- route_ids: int32 [1024, 2], P('sp'), may hold values from 0 to 7, all different within a row; in each aligned block of 128 rows (0 to 127, 128 to 255, ...) at most 48 rows name the same one
- route_weight: float32 [1024, 2], P('sp'), may hold values from 0.25 to 2.25
- expert_gate: bfloat16 [8, 2048, 2048], P('sp', None, 'tp'), may hold values from -0.125 to 0.125
- expert_up: bfloat16 [8, 2048, 2048], P('sp', None, 'tp'), may hold values from -0.125 to 0.125
- expert_down: bfloat16 [8, 2048, 2048], P('sp', 'tp'), may hold values from -0.125 to 0.125
- out_proj: bfloat16 [2048, 4096], P('sp', 'tp'), may hold values from -0.09375 to 0.09375
- mixed: bfloat16 [1024, 4096], P('sp', 'tp'), may hold values from -6 to 6
- query: bfloat16 [1024, 2048], P('sp', 'tp'), may hold values from -6 to 6
- key: bfloat16 [1024, 2048], P('sp', 'tp'), may hold values from -1.5 to 1.5
- value: bfloat16 [1024, 4096], P('sp', 'tp'), may hold values from -6 to 6
- log_decay: float32 [1024, 2048], P('sp', 'tp'), may hold values from -1 to 0, as said below
- span_state: float32 [8, 16, 128, 256], P('sp', 'tp'), may hold values from -24 to 24
Outputs:
- grad_expert_gate: bfloat16 [8, 2048, 2048], P('sp', None, 'tp')
- grad_expert_up: bfloat16 [8, 2048, 2048], P('sp', None, 'tp')
- grad_expert_down: bfloat16 [8, 2048, 2048], P('sp', 'tp')
- grad_out_proj: float32 [2048, 4096], P('sp', 'tp')
- grad_query: bfloat16 [1024, 2048], P('sp', 'tp')
- grad_key: bfloat16 [1024, 2048], P('sp', 'tp')
- grad_value: bfloat16 [1024, 4096], P('sp', 'tp')
- grad_log_decay: float32 [1024, 2048], P('sp', 'tp')
Inputs may be any that keep to these rules, and one draw needn't show every extreme that they name: `route_ids`: A row names 2 different experts. Within each aligned block of 128 rows (the rows of one index of sp) no expert is named by more than 48 rows, and in every draw some expert is named by exactly 48 rows of some block. `log_decay`: every entry is zero or negative.
All inputs are finite; a program needn't handle non-finite values.
Results may differ from a plain program's by a relative error of at most 0.023.
Values may be sent and summed in bfloat16 or wider, within the bound.
A program may use at most 128 MiB of HBM per device.

v0:
```python
import jax
import jax.numpy as jnp
from jax import lax
from jax.sharding import PartitionSpec as P

KEY_CHANNELS = 128
DV = 256
TOP = 2
BLOCK = 64
epsilon = 1e-06
highest = lax.Precision.HIGHEST


def entering(array, axis, join, neutral):
    count = lax.axis_size(axis)
    place = lax.axis_index(axis)
    ahead = count - 1 - place
    gathered = jax.tree.map(
        lambda a, kind: lax.all_gather(a.astype(kind), axis), array, (jnp.bfloat16, jnp.bfloat16)
    )
    state = jax.tree.map(lambda a, e: jnp.zeros_like(a) + jnp.asarray(e, a.dtype), array, neutral)

    def one(lap, state):
        source = count - 1 - lap
        return join(
            state,
            jax.tree.map(
                lambda a, own: lax.dynamic_index_in_dim(a, source, 0, False).astype(own.dtype),
                gathered,
                array,
            ),
        )

    return lax.fori_loop(0, ahead, one, state)


def into_blocks(values):
    return values.reshape(values.shape[0] // BLOCK, BLOCK, values.shape[1])


def span_forward(query_rows, key_rows, value_rows, grad_rows, decay_rows, entry_state):
    query_blk = into_blocks(query_rows)
    key_blk = into_blocks(key_rows)
    value_blk = into_blocks(value_rows)
    grad_blk = into_blocks(grad_rows)
    cumlog = jnp.cumsum(into_blocks(decay_rows), axis=1)
    block_total = cumlog[:, -1, :]
    to_end = jnp.exp(block_total[:, None, :] - cumlog)
    inner_part = jnp.einsum("nsd,nsj->ndj", key_blk * to_end, value_blk, precision=highest)

    def forward_step(carry_state, step_item):
        piece_part, block_sum = step_item
        return (jnp.exp(block_sum)[:, None] * carry_state + piece_part, carry_state)

    end_state, starts = lax.scan(forward_step, entry_state, (inner_part, block_total))
    own_part = jnp.einsum("ntd,ntj->ndj", query_blk * jnp.exp(cumlog), grad_blk, precision=highest)

    def backward_step(carry_state, step_item):
        piece_part, block_sum = step_item
        return (jnp.exp(block_sum)[:, None] * carry_state + piece_part, carry_state)

    start_cot, after_cot = lax.scan(
        backward_step, jnp.zeros_like(entry_state), (own_part, block_total), reverse=True
    )
    span_total = jnp.sum(block_total, axis=0)
    later_log = span_total[None, :] - jnp.cumsum(block_total, axis=0)
    return ((cumlog, starts, after_cot, later_log, end_state), (jnp.exp(span_total), start_cot))


def span_backward(query_rows, key_rows, value_rows, grad_rows, kept_terms, exit_cot):
    cumlog, starts, after_cot, later_log, end_state = kept_terms
    query_blk = into_blocks(query_rows)
    key_blk = into_blocks(key_rows)
    value_blk = into_blocks(value_rows)
    grad_blk = into_blocks(grad_rows)
    exit_cots = after_cot + jnp.exp(later_log)[:, :, None] * exit_cot
    causal = jnp.arange(BLOCK)[:, None] >= jnp.arange(BLOCK)[None, :]
    decays = jnp.exp(
        jnp.where(causal[None, :, :, None], cumlog[:, :, None, :] - cumlog[:, None, :, :], -jnp.inf)
    )
    scores = jnp.einsum("ntd,nsd,ntsd->nts", query_blk, key_blk, decays, precision=highest)
    grad_scores = jnp.einsum("ntj,nsj->nts", grad_blk, value_blk, precision=highest)
    grad_query = jnp.exp(cumlog) * jnp.einsum("ntj,ndj->ntd", grad_blk, starts, precision=highest)
    grad_query = grad_query + jnp.einsum(
        "nts,nsd,ntsd->ntd", grad_scores, key_blk, decays, precision=highest
    )
    to_end = jnp.exp(cumlog[:, -1:, :] - cumlog)
    grad_key = jnp.einsum("nts,ntd,ntsd->nsd", grad_scores, query_blk, decays, precision=highest)
    grad_key = grad_key + to_end * jnp.einsum(
        "nsj,ndj->nsd", value_blk, exit_cots, precision=highest
    )
    grad_value = jnp.einsum("nts,ntj->nsj", scores, grad_blk, precision=highest)
    grad_value = grad_value + jnp.einsum(
        "nsd,ndj->nsj", key_blk * to_end, exit_cots, precision=highest
    )
    length = query_rows.shape[0]
    key_width = query_rows.shape[1]
    per_position = (query_blk * grad_query - key_blk * grad_key).reshape(length, key_width)
    grad_log = (
        jnp.flip(jnp.cumsum(jnp.flip(per_position, 0), 0), 0)
        + jnp.sum(end_state * exit_cot, axis=1)[None, :]
    )
    return (
        grad_query.reshape(length, key_width),
        grad_key.reshape(length, key_width),
        grad_value.reshape(length, value_rows.shape[1]),
        grad_log,
    )


def join_later(earlier, later):
    return (earlier[0] * later[0], later[1] + later[0][..., None] * earlier[1])


def on_device(
    resid,
    norm_gain,
    cotangent,
    route_ids,
    route_weight,
    expert_gate,
    expert_up,
    expert_down,
    out_proj,
    mixed,
    query,
    key,
    value,
    log_decay,
    span_state,
):
    tokens_here = resid.shape[0]
    model_width = resid.shape[1]
    sp_count = lax.axis_size("sp")
    tp_count = lax.axis_size("tp")
    experts = sp_count * expert_gate.shape[0]
    capacity = 3 * tokens_here // experts
    resid_f = resid.astype(jnp.float32)
    inverse_rms = lax.rsqrt(jnp.mean(resid_f * resid_f, axis=1, keepdims=True) + epsilon)
    unit_rows = resid_f * inverse_rms
    normed = (unit_rows * norm_gain).astype(jnp.bfloat16)
    pair_expert = route_ids.reshape(-1)
    onehot = (pair_expert[:, None] == jnp.arange(experts, dtype=jnp.int32)[None, :]).astype(
        jnp.int32
    )
    slot_rank = jnp.sum((jnp.cumsum(onehot, axis=0) - onehot) * onehot, axis=1)
    slot_of = pair_expert * capacity + slot_rank
    slot_pairs = slot_of[None, :] == jnp.arange(experts * capacity, dtype=jnp.int32)[:, None]
    slot_tokens = jnp.any(slot_pairs.reshape(experts * capacity, tokens_here, TOP), axis=2).astype(
        jnp.bfloat16
    )
    slot_weight = jnp.sum(jnp.where(slot_pairs, route_weight.reshape(1, -1), 0.0), axis=1)
    column_share = model_width // tp_count
    offset = lax.axis_index("tp") * column_share
    rows_in = jnp.dot(
        slot_tokens,
        lax.dynamic_slice_in_dim(normed, offset, column_share, 1),
        preferred_element_type=jnp.float32,
    ).astype(jnp.bfloat16)
    rows_cot = (
        jnp.dot(
            slot_tokens,
            lax.dynamic_slice_in_dim(cotangent, offset, column_share, 1),
            preferred_element_type=jnp.float32,
        )
        * slot_weight[:, None]
    )
    arrived = (
        lax.all_to_all(
            rows_in.reshape(experts, capacity, -1), "sp", split_axis=0, concat_axis=1, tiled=True
        ),
        lax.all_to_all(
            rows_cot.astype(jnp.bfloat16).reshape(experts, capacity, -1),
            "sp",
            split_axis=0,
            concat_axis=1,
            tiled=True,
        ),
    )
    expert_in, expert_cot = (
        lax.all_gather(arrived[0], "tp", axis=2, tiled=True),
        lax.all_gather(arrived[1], "tp", axis=2, tiled=True),
    )
    gate_pre = jnp.einsum(
        "erd,edf->erf", expert_in, expert_gate, preferred_element_type=jnp.float32
    )
    up_pre = jnp.einsum("erd,edf->erf", expert_in, expert_up, preferred_element_type=jnp.float32)
    gate_sig = jax.nn.sigmoid(gate_pre)
    hidden = (gate_pre * gate_sig * up_pre).astype(jnp.bfloat16)
    grad_hidden = jnp.einsum(
        "erd,efd->erf", expert_cot, expert_down, preferred_element_type=jnp.float32
    )
    grad_up_act = (grad_hidden * gate_pre * gate_sig).astype(jnp.bfloat16)
    grad_gate_act = (grad_hidden * up_pre * gate_sig * (1.0 + gate_pre * (1.0 - gate_sig))).astype(
        jnp.bfloat16
    )
    grad_down_w = jnp.einsum("erf,erd->efd", hidden, expert_cot, preferred_element_type=jnp.float32)
    grad_gate_w = jnp.einsum(
        "erd,erf->edf", expert_in, grad_gate_act, preferred_element_type=jnp.float32
    )
    grad_up_w = jnp.einsum(
        "erd,erf->edf", expert_in, grad_up_act, preferred_element_type=jnp.float32
    )
    partial_value = jnp.einsum(
        "erf,edf->erd", grad_gate_act, expert_gate, preferred_element_type=jnp.float32
    )
    partial_value = partial_value + jnp.einsum(
        "erf,edf->erd", grad_up_act, expert_up, preferred_element_type=jnp.float32
    )
    partial_short = partial_value.astype(jnp.bfloat16)
    summed = (
        lax.psum_scatter(partial_short, "tp", scatter_dimension=2, tiled=True)
        .astype(jnp.float32)
        .astype(jnp.bfloat16)
    )
    returned = lax.all_to_all(summed, "sp", split_axis=1, concat_axis=0, tiled=True)
    flat_rows = returned.reshape(experts * capacity, -1)
    grad_normed = lax.all_gather(
        lax.dot_general(
            slot_tokens, flat_rows, (((0,), (0,)), ((), ())), preferred_element_type=jnp.float32
        ).astype(jnp.bfloat16),
        "tp",
        axis=1,
        tiled=True,
    ).astype(jnp.float32)
    scaled = grad_normed * norm_gain
    grad_resid = cotangent.astype(jnp.float32) + inverse_rms * (
        scaled - unit_rows * jnp.mean(scaled * unit_rows, axis=1, keepdims=True)
    )
    grad_resid = grad_resid.astype(jnp.bfloat16)
    resid_cols = grad_resid
    grad_out_proj = lax.psum_scatter(
        lax.dot_general(
            resid_cols, mixed, (((0,), (0,)), ((), ())), preferred_element_type=jnp.float32
        ).astype(jnp.bfloat16),
        "sp",
        scatter_dimension=0,
        tiled=True,
    ).astype(jnp.float32)
    resid_cols = grad_resid
    grad_mixed = jnp.dot(
        resid_cols,
        lax.all_gather(out_proj, "sp", axis=0, tiled=True),
        preferred_element_type=jnp.float32,
    ).astype(jnp.bfloat16)
    head_count = query.shape[1] // KEY_CHANNELS
    query_scale = KEY_CHANNELS ** (-0.5)

    def heads_first(values, head_depth):
        return values.reshape(tokens_here, head_count, head_depth).transpose(1, 0, 2)

    query_rows = heads_first(query, KEY_CHANNELS).astype(jnp.float32) * query_scale
    key_rows = heads_first(key, KEY_CHANNELS).astype(jnp.float32)
    value_rows = heads_first(value, DV).astype(jnp.float32)
    grad_rows = heads_first(grad_mixed, DV).astype(jnp.float32)
    decay_rows = heads_first(log_decay, KEY_CHANNELS)
    kept_terms, summary = jax.vmap(span_forward)(
        query_rows, key_rows, value_rows, grad_rows, decay_rows, span_state[0]
    )
    identity = (jnp.ones_like(summary[0]), jnp.zeros_like(summary[1]))
    carried = entering((summary[0], summary[1]), "sp", join_later, identity)
    head_grads = jax.vmap(span_backward)(
        query_rows, key_rows, value_rows, grad_rows, kept_terms, carried[1]
    )

    def tokens_first(values):
        return values.transpose(1, 0, 2).reshape(tokens_here, -1)

    grad_query = (tokens_first(head_grads[0]) * query_scale).astype(jnp.bfloat16)
    grad_key = tokens_first(head_grads[1]).astype(jnp.bfloat16)
    grad_value = tokens_first(head_grads[2]).astype(jnp.bfloat16)
    grad_log_decay = tokens_first(head_grads[3])
    return (
        grad_gate_w.astype(jnp.bfloat16),
        grad_up_w.astype(jnp.bfloat16),
        grad_down_w.astype(jnp.bfloat16),
        grad_out_proj,
        grad_query,
        grad_key,
        grad_value,
        grad_log_decay,
    )


def solution(mesh):
    return jax.shard_map(
        on_device,
        mesh=mesh,
        in_specs=(
            P("sp", None),
            P(),
            P("sp", None),
            P("sp", None),
            P("sp", None),
            P("sp", None, "tp"),
            P("sp", None, "tp"),
            P("sp", "tp", None),
            P("sp", "tp"),
            P("sp", "tp"),
            P("sp", "tp"),
            P("sp", "tp"),
            P("sp", "tp"),
            P("sp", "tp"),
            P("sp", "tp", None, None),
        ),
        out_specs=(
            P("sp", None, "tp"),
            P("sp", None, "tp"),
            P("sp", "tp", None),
            P("sp", "tp"),
            P("sp", "tp"),
            P("sp", "tp"),
            P("sp", "tp"),
            P("sp", "tp"),
        ),
        check_vma=False,
    )
```

profile of v0, /device:TPU:0, one launch (start us, length us, event | category | flops | bytes accessed | tf_op | source)
XLA Modules:
  0.0 320.2 jit_solution(13305534653315224760)
XLA Ops:
  11.3 1.2 fusion.27
  12.6 1.1 convert_multiply_fusion
  13.8 1.2 convolution_convert_fusion.4
  15.0 19.2 %all_to_all.33 = bf16[8,48,512]{2,1,0:T(8,128)(2,1)} all-to-all(bf16[8,48,512]{2,1,0:T(8,128)(2,1)S(1)} %bitcast.230), channel_id=1, replica_groups=mesh['sp'=8,'tp'=4] {'sp'}, dimensions={0} | all-to-all | bytes 786432 | tf_op jit(solution)/shard_map/all_to_all | solution.py:169
  35.0 15.1 %all_to_all.34 = bf16[8,48,512]{2,1,0:T(8,128)(2,1)} all-to-all(bf16[8,48,512]{2,1,0:T(8,128)(2,1)S(1)} %bitcast.231), channel_id=1, replica_groups=mesh['sp'=8,'tp'=4] {'sp'}, dimensions={0} | all-to-all | bytes 786432 | tf_op jit(solution)/shard_map/all_to_all | solution.py:172
  50.2 2.6 all-gather.8.cloned.1.call-done
  52.7 4.0 %fusion.12 = f32[384,512]{1,0:T(8,128)} fusion(bf16[1,2048,512]{2,1,0:T(8,128)(2,1)} %param.27, bf16[1,384,2048]{2,1,0:T(8,128)(2,1)} %all-gather.8.cloned.1.call-done), kind=kOutput, calls=%fused_computation.29 | convolution fusion | flops 805306368 | bytes 4456448 | tf_op jit(solution)/shard_map/erd,edf->erf/dot_general | solution.py:187
  56.8 1.9 fusion.9
  58.6 15.3 %all-gather.10.cloned.1.call-done = bf16[1,384,2048]{2,1,0:T(8,128)(2,1)} async-done(((bf16[1,384,512]{2,1,0:T(8,128)(2,1)}), bf16[1,384,2048]{2,1,0:T(8,128)(2,1)}) %all-gather.10.cloned.1.call-update) | async-done | bytes 1572880 | tf_op jit(solution)/shard_map/all_gather | solution.py:182
  74.0 3.7 %multiply_convert_fusion.1 = (bf16[384,512]{1,0:T(8,128)(2,1)S(1)}, bf16[384,512]{1,0:T(8,128)(2,1)S(1)}) fusion(f32[384,512]{1,0:T(8,128)} %fusion.9, f32[384,512]{1,0:T(8,128)} %fusion.12, bf16[1,512,2048]{2,1,0:T(8,128)(2,1)} %param.28, bf16[1,384,2048]{2,1,0:T(8,128)(2,1)} %all-gather.10.cloned.1.call-done), kind=kOutput, calls=%fused_computation.64 | convolution fusion | flops 807862272 | bytes 6029312 | tf_op jit(solution)/shard_map/erd,efd->erf/dot_general | solution.py:190
  77.7 1.0 fusion.7
  79.5 2.2 fusion.6
  82.3 27.6 %reduce-scatter.3.cloned.1.call-done = bf16[1,384,512]{2,1,0:T(8,128)(2,1)} async-done(((bf16[1,384,2048]{2,1,0:T(8,128)(2,1)}), bf16[1,384,512]{2,1,0:T(8,128)(2,1)}) %reduce-scatter.3.cloned.1.call-update) | async-done | bytes 393232 | tf_op jit(solution)/shard_map/reduce_scatter | solution.py:212
  109.9 1.6 copy.278
  112.0 3.0 reduce.9
  115.0 1.0 reshape.320
  116.1 5.6 %all-to-all-start.2 = ((bf16[8,2,12288]{2,1,0:T(2,128)(2,1)}), bf16[8,2,12288]{2,1,0:T(2,128)(2,1)S(1)}, u32[]{:S(2)}, u32[]{:S(2)}) async-start(bf16[8,2,12288]{2,1,0:T(2,128)(2,1)} %reshape.320), calls=%async_computation.3 | async-start | bytes 786432 | tf_op jit(solution)/shard_map/all_to_all | solution.py:216
  123.5 21.2 %all-to-all-done.2 = bf16[8,2,12288]{2,1,0:T(2,128)(2,1)S(1)} async-done(((bf16[8,2,12288]{2,1,0:T(2,128)(2,1)}), bf16[8,2,12288]{2,1,0:T(2,128)(2,1)S(1)}, u32[]{:S(2)}, u32[]{:S(2)}) %all-to-all-start.2) | async-done | bytes 393248 | tf_op jit(solution)/shard_map/all_to_all | solution.py:216
  145.4 6.9 %all_gather.24 = bf16[128,2048]{1,0:T(8,128)(2,1)S(1)} all-gather(bf16[128,512]{1,0:T(8,128)(2,1)S(1)} %convolution_convert_fusion.6), channel_id=1, replica_groups=mesh['sp'=8,'tp'=4] {'tp'}, dimensions={1}, use_global_device_ids=true | all-gather | bytes 655360 | tf_op jit(solution)/shard_map/all_gather | solution.py:218
  153.3 10.2 %all-gather.12.cloned.1.call-done = bf16[2048,1024]{1,0:T(8,128)(2,1)} async-done(((bf16[256,1024]{1,0:T(8,128)(2,1)}), bf16[2048,1024]{1,0:T(8,128)(2,1)}) %all-gather.12.cloned.1.call-update) | async-done | bytes 4194320 | tf_op jit(solution)/shard_map/all_gather | solution.py:243
  163.5 3.1 convolution_convert_fusion.5
  166.8 1.6 convolution_bitcast_fusion
  168.4 1.1 broadcast.91.clone.1
  169.5 2.1 while.45
  172.4 1.2 reshape.289
  174.3 19.4 %all-gather.2 = bf16[8,4,128]{2,1,0:T(4,128)(2,1)} all-gather(bf16[1,4,128]{2,1,0:T(4,128)(2,1)S(1)} %fusion.47), channel_id=3, replica_groups=mesh['sp'=8,'tp'=4] {'sp'}, dimensions={0}, use_global_device_ids=true | all-gather | bytes 9216 | tf_op jit(solution)/shard_map/all_gather | solution.py:19
  195.8 4.5 %convolution_convert_fusion = bf16[2048,1024]{1,0:T(8,128)(2,1)} fusion(bf16[128,1024]{1,0:T(8,128)(2,1)S(1)} %copy-done.25, bf16[128,2048]{1,0:T(8,128)(2,1)S(1)} %all_gather.24, bf16[128,2048]{1,0:T(8,128)(2,1)} %param.23, f32[128]{0:T(128)} %copy-done.30, f32[2048]{0:T(1024)S(1)} %copy-done.26, f32[128]{0:T(128)} %copy-done.29, ...), kind=kOutput, calls=%fused_computation.15 | convolution fusion | flops 541589504 | bytes 6038528 | tf_op jit(solution)/shard_map/dot_general | solution.py:233
  201.3 9.4 %fusion = (f32[4,2,64,64]{3,2,1,0:T(8,128)}, f32[4,2,64,128,64]{3,4,2,1,0:T(8,128)}) fusion(f32[4,2,128,64]{2,3,1,0:T(8,128)S(1)} %bitcast.214, f32[4,2,128,64]{2,3,1,0:T(8,128)S(1)} %bitcast.226, f32[4,2,64,128]{3,2,1,0:T(8,128)S(1)} %reduce_window_sum.50, pred[64,64]{1,0:T(8,128)(4,1)S(1)} %iota_compare_fusion.2), kind=kLoop, calls=%fused_computation.9 | loop fusion | flops 20938752 | bytes 17698816 | tf_op jit(solution)/shard_map/vmap(ntd,nsd,ntsd->nts)/dot_general | solution.py:81
  211.3 4.5 %fusion.4 = bf16[1,2048,512]{2,1,0:T(8,128)(2,1)} fusion(bf16[384,512]{1,0:T(8,128)(2,1)} %copy-done.21, bf16[1,384,2048]{2,1,0:T(8,128)(2,1)} %all-gather.8.cloned.1.call-done), kind=kOutput, calls=%fused_computation.21 | convolution fusion | flops 806354944 | bytes 4063232 | tf_op jit(solution)/shard_map/erd,erf->edf/dot_general | solution.py:201
  215.9 2.6 fusion.3
  218.5 2.7 fusion.5
  221.5 1.2 fusion.52
  222.8 15.1 %fusion.1 = f32[4,2,64,128]{3,2,1,0:T(8,128)S(1)} fusion(f32[4,2,64,128,64]{3,4,2,1,0:T(8,128)} %get-tuple-element.416, f32[4,2,64,128]{3,2,1,0:T(8,128)S(1)} %bitcast.215, f32[4,2,64,64]{3,2,1,0:T(8,128)S(1)} %copy.217), kind=kLoop, calls=%fused_computation.11 | loop fusion | flops 12517376 | bytes 17432576 | tf_op jit(solution)/shard_map/vmap(nts,nsd,ntsd->ntd)/dot_general | solution.py:84
  237.9 1.4 fusion.26
  239.4 6.3 %multiply_reduce_fusion = f32[4,2,64,128]{3,2,1,0:T(8,128)} fusion(f32[4,2,64,64]{3,2,1,0:T(8,128)S(1)} %fusion.51, f32[4,2,64,128]{3,2,1,0:T(8,128)S(1)} %bitcast.227, f32[4,2,64,128]{3,2,1,0:T(8,128)S(1)} %reduce_window_sum.50, pred[64,64]{1,0:T(8,128)(4,1)S(1)} %iota_compare_fusion.2), kind=kLoop, calls=%fused_computation.12 | loop fusion | flops 20905984 | bytes 921600 | tf_op jit(solution)/shard_map/vmap(nts,ntd,ntsd->nsd)/dot_general | solution.py:88
  245.8 12.8 %while.44 = (s32[]{:T(128)}, f32[4,128,256]{2,1,0:T(8,128)S(1)}, s32[]{:T(128)}, bf16[8,4,128,256]{3,2,1,0:T(8,128)(2,1)}, bf16[8,4,128]{2,1,0:T(4,128)(2,1)}, /*index=5*/s32[]{:T(128)}, s32[]{:T(128)}, s32[]{:T(128)}, s32[]{:T(128)}) while((s32[]{:T(128)}, f32[4,128,256]{2,1,0:T(8,128)S(1)}, s32[]{:T(128)}, ...), condition=%wide.region_17.18_spmd, body=%wide.region_16.17_spmd.sunk | while | flops 393734 | bytes 1315987 | solution.py:34
  246.5 1.1 convert_add_fusion.2
  248.2 1.1 convert_add_fusion.2
  250.0 1.1 convert_add_fusion.2
  251.9 1.1 convert_add_fusion.2
  253.7 1.1 convert_add_fusion.2
  255.4 1.1 convert_add_fusion.2
  257.3 1.1 convert_add_fusion.2
  258.6 2.7 multiply_subtract_fusion
  261.3 1.7 rev.7
  264.6 2.3 fusion.23
  268.3 42.4 %reduce-scatter.5.cloned.1.call-done = bf16[256,1024]{1,0:T(8,128)(2,1)} async-done(((bf16[2048,1024]{1,0:T(8,128)(2,1)}), bf16[256,1024]{1,0:T(8,128)(2,1)}) %reduce-scatter.5.cloned.1.call-update) | async-done | bytes 524304 | tf_op jit(solution)/shard_map/reduce_scatter | solution.py:232
  310.7 2.1 convert_element_type.191
  (164 shorter events, 25.4 us)
Async XLA Ops:
  8.0 48.8 %copy-start = (bf16[1,2048,512]{2,1,0:T(8,128)(2,1)S(1)}, bf16[1,2048,512]{2,1,0:T(8,128)(2,1)}, u32[]{:S(2)}) copy-start(bf16[1,2048,512]{2,1,0:T(8,128)(2,1)} %param.26) | copy-start | bytes 6291460
  8.0 4.5 %copy-start.3 = (bf16[128,2048]{1,0:T(8,128)(2,1)S(1)}, bf16[128,2048]{1,0:T(8,128)(2,1)}, u32[]{:S(2)}) copy-start(bf16[128,2048]{1,0:T(8,128)(2,1)} %param.21) | copy-start | bytes 1572868
  8.0 5.7 %copy-start.26 = (f32[2048]{0:T(1024)S(1)}, f32[2048]{0:T(1024)}, u32[]{:S(2)}) copy-start(f32[2048]{0:T(1024)} %param.22) | copy-start | bytes 24580
  8.0 44.7 %all-gather.8.cloned.1.call-start = ((), (), s32[]{:S(2)}) async-start(), calls=%async_computation.5 | async-start | bytes 1966080 | tf_op jit(solution)/shard_map/all_gather | solution.py:181
  10.2 24.1 %copy-start.31 = (f32[128,2]{0,1:T(2,128)S(1)}, f32[128,2]{0,1:T(2,128)}, u32[]{:S(2)}) copy-start(f32[128,2]{0,1:T(2,128)} %param.25) | copy-start | bytes 3076
  10.5 24.2 %copy-start.9 = (bf16[128,2048]{1,0:T(8,128)(2,1)S(1)}, bf16[128,2048]{1,0:T(8,128)(2,1)}, u32[]{:S(2)}) copy-start(bf16[128,2048]{1,0:T(8,128)(2,1)} %param.23) | copy-start | bytes 1572868
  11.3 23.7 %copy-start.19 = (pred[384,128]{1,0:T(8,128)(4,1)}, pred[384,128]{1,0:T(8,128)(4,1)S(1)}, u32[]{:S(2)}) copy-start(pred[384,128]{1,0:T(8,128)(4,1)S(1)} %fusion.34) | copy-start | bytes 147460
  12.6 1.1 copy-start.29
  34.2 39.7 %all-gather.10.cloned.1.call-start = ((), (), s32[]{:S(2)}) async-start(), calls=%async_computation.6 | async-start | bytes 1966080 | tf_op jit(solution)/shard_map/all_gather | solution.py:182
  50.1 59.7 %reduce-scatter.3.cloned.1.call-start = ((), (), s32[]{:S(2)}) async-start(), calls=%async_computation.7 | async-start | bytes 1966080 | tf_op jit(solution)/shard_map/reduce_scatter | solution.py:212
  52.7 4.0 %copy-start.32 = (bf16[1,384,2048]{2,1,0:T(8,128)(2,1)S(1)}, bf16[1,384,2048]{2,1,0:T(8,128)(2,1)}, u32[]{:S(2)}) copy-start(bf16[1,384,2048]{2,1,0:T(8,128)(2,1)} %all-gather.8.cloned.1.call-done) | copy-start | bytes 4718596
  77.6 1.0 copy-start.22
  77.7 1.0 copy-start.21
  77.7 1.9 copy-start.12
  81.7 81.7 %all-gather.12.cloned.1.call-start = ((), (), s32[]{:S(2)}) async-start(), calls=%async_computation.9 | async-start | bytes 4718592 | tf_op jit(solution)/shard_map/all_gather | solution.py:243
  82.3 39.5 %copy-start.24 = (f32[128,512]{1,0:T(8,128)S(1)}, f32[128,512]{1,0:T(8,128)}, u32[]{:S(2)}) copy-start(f32[128,512]{1,0:T(8,128)} %param.34) | copy-start | bytes 786436
  112.0 10.8 %copy-start.17 = (bf16[128,512]{1,0:T(8,128)(2,1)S(1)}, bf16[128,512]{1,0:T(8,128)(2,1)}, u32[]{:S(2)}) copy-start(bf16[128,512]{1,0:T(8,128)(2,1)} %param.31) | copy-start | bytes 393220
  116.1 29.0 %copy-start.20 = (pred[384,128]{1,0:T(8,128)(4,1)S(1)}, pred[384,128]{1,0:T(8,128)(4,1)}, u32[]{:S(2)}) copy-start(pred[384,128]{1,0:T(8,128)(4,1)} %copy-done.19) | copy-start | bytes 147460
  116.1 28.6 %all-to-all-start.2 = ((bf16[8,2,12288]{2,1,0:T(2,128)(2,1)}), bf16[8,2,12288]{2,1,0:T(2,128)(2,1)S(1)}, u32[]{:S(2)}, u32[]{:S(2)}) async-start(bf16[8,2,12288]{2,1,0:T(2,128)(2,1)} %reshape.320), calls=%async_computation.3 | async-start | bytes 786432 | tf_op jit(solution)/shard_map/all_to_all | solution.py:216
  121.7 124.0 %all-gather.14.cloned.1.call-start = ((), (), s32[]{:S(2)}) async-start(), calls=%async_computation.10 | async-start | bytes 2359296 | tf_op jit(solution)/shard_map/all_gather | solution.py:19
  153.3 13.3 %copy-start.30 = (f32[128]{0:T(128)}, f32[128]{0:T(128)S(1)}, u32[]{:S(2)}) copy-start(f32[128]{0:T(128)S(1)} %broadcast_multiply_fusion) | copy-start | bytes 1540
  171.6 2.1 copy-start.28
  171.6 22.1 %copy-start.16 = (bf16[128,512]{1,0:T(8,128)(2,1)S(1)}, bf16[128,512]{1,0:T(8,128)(2,1)}, u32[]{:S(2)}) copy-start(bf16[128,512]{1,0:T(8,128)(2,1)} %param.32) | copy-start | bytes 393220
  172.3 23.5 %copy-start.25 = (bf16[128,1024]{1,0:T(8,128)(2,1)S(1)}, bf16[128,1024]{1,0:T(8,128)(2,1)}, u32[]{:S(2)}) copy-start(bf16[128,1024]{1,0:T(8,128)(2,1)} %param.30) | copy-start | bytes 786436
  172.4 138.4 %reduce-scatter.5.cloned.1.call-start = ((), (), s32[]{:S(2)}) async-start(), calls=%async_computation.8 | async-start | bytes 4718592 | tf_op jit(solution)/shard_map/reduce_scatter | solution.py:232
  173.6 26.7 %copy-start.5 = (bf16[4,128,256]{2,1,0:T(8,128)(2,1)}, bf16[4,128,256]{2,1,0:T(8,128)(2,1)S(1)}, u32[]{:S(2)}) copy-start(bf16[4,128,256]{2,1,0:T(8,128)(2,1)S(1)} %copy.213) | copy-start | bytes 786436
  200.3 1.0 copy-start.10
  201.3 9.5 %copy-start.2 = (f32[1,4,128,256]{3,2,1,0:T(8,128)S(1)}, f32[1,4,128,256]{3,2,1,0:T(8,128)}, u32[]{:S(2)}) copy-start(f32[1,4,128,256]{3,2,1,0:T(8,128)} %param.35) | copy-start | bytes 1572868
  211.2 4.6 %copy-start.7 = (f32[2,4,128,256]{3,2,1,0:T(8,128)}, f32[2,4,128,256]{3,2,1,0:T(8,128)S(1)}, u32[]{:S(2)}) copy-start(f32[2,4,128,256]{3,2,1,0:T(8,128)S(1)} %get-tuple-element.224) | copy-start | bytes 3145732
  211.3 4.6 %copy-start.23 = (bf16[384,512]{1,0:T(8,128)(2,1)S(1)}, bf16[384,512]{1,0:T(8,128)(2,1)}, u32[]{:S(2)}) copy-start(bf16[384,512]{1,0:T(8,128)(2,1)} %copy-done.22) | copy-start | bytes 1179652
  211.3 4.6 %copy-start.33 = (bf16[1,384,2048]{2,1,0:T(8,128)(2,1)S(1)}, bf16[1,384,2048]{2,1,0:T(8,128)(2,1)}, u32[]{:S(2)}) copy-start(bf16[1,384,2048]{2,1,0:T(8,128)(2,1)} %all-gather.8.cloned.1.call-done) | copy-start | bytes 4718596
  215.8 2.7 copy-start.34
  215.8 2.7 copy-start.35
  215.8 2.7 copy-start.36
  218.5 2.7 copy-start.6
  218.5 3.0 copy-start.13
  222.8 15.1 %copy-start.8 = (f32[2,4,128,256]{3,2,1,0:T(8,128)S(1)}, f32[2,4,128,256]{3,2,1,0:T(8,128)}, u32[]{:S(2)}) copy-start(f32[2,4,128,256]{3,2,1,0:T(8,128)} %copy-done.7) | copy-start | bytes 3145732
  237.9 1.5 copy-start.11
  239.4 19.2 %copy-start.15 = (f32[16,4,8,128]{3,2,1,0:T(8,128)S(1)}, f32[16,4,8,128]{3,2,1,0:T(8,128)}, u32[]{:S(2)}) copy-start(f32[16,4,8,128]{3,2,1,0:T(8,128)} %multiply_bitcast_fusion) | copy-start | bytes 786436
  245.7 12.9 %copy-start.4 = (f32[2,4,128,256]{3,2,1,0:T(8,128)S(1)}, f32[2,4,128,256]{3,2,1,0:T(8,128)}, u32[]{:S(2)}) copy-start(f32[2,4,128,256]{3,2,1,0:T(8,128)} %get-tuple-element.225) | copy-start | bytes 3145732
  245.7 12.9 %copy-start.14 = (f32[16,4,8,128]{3,2,1,0:T(8,128)S(1)}, f32[16,4,8,128]{3,2,1,0:T(8,128)}, u32[]{:S(2)}) copy-start(f32[16,4,8,128]{3,2,1,0:T(8,128)} %convert_bitcast_fusion) | copy-start | bytes 786436
  245.7 12.9 %copy-start.27 = (f32[4,2,128]{2,0,1:T(4,128)S(1)}, f32[4,2,128]{2,0,1:T(4,128)}, u32[]{:S(2)}) copy-start(f32[4,2,128]{2,0,1:T(4,128)} %copy.222) | copy-start | bytes 12292
  263.7 49.1 %copy-start.1 = (bf16[1,2048,512]{2,1,0:T(8,128)(2,1)S(1)}, bf16[1,2048,512]{2,1,0:T(8,128)(2,1)}, u32[]{:S(2)}) copy-start(bf16[1,2048,512]{2,1,0:T(8,128)(2,1)} %param.26) | copy-start | bytes 6291460
  264.6 3.0 copy-start.18
Sparse Core Ops, SparseCore 0:
  34.4 18.3 all-gather.7
  54.3 19.6 all-gather.9
  81.8 27.9 reduce-scatter.2
Sparse Core Ops, SparseCore 1:
  84.3 79.1 all-gather.11
  172.4 47.9 all-gather.13
  223.9 86.8 reduce-scatter.4
where the time goes:
time: 321 us; the launch traced here: 320 us
  waiting for transfers between devices  120 us (37%)
  blocking collectives  60.6 us (19%)
  other arithmetic  60 us (19%)
  matrix products  42 us (13%)
  between operations  16.1 us (5%)
  local copies, waits for them, and re-layouts  15.2 us (5%)
  starting transfers between devices  5.89 us (2%)
    reduce_scatter x1, waiting for transfers between devices, on_device(): lax.psum_scatter(lax.dot_general(resid_cols, mixed, (((0,), (0,)), ((), (...  42.4 us
    reduce_scatter x1, waiting for transfers between devices, on_device(): lax.psum_scatter(partial_short, 'tp', scatter_dimension=2, tiled=True)  27.6 us
    all_to_all x1, waiting for transfers between devices, on_device(): lax.all_to_all(summed, 'sp', split_axis=1, concat_axis=0, tiled=True)  21.2 us
    all_gather x1, blocking collectives, entering(): lax.all_gather(a.astype(kind), axis)  19.4 us
    all_to_all x1, blocking collectives, on_device(): lax.all_to_all(rows_in.reshape(experts, capacity, -1), 'sp', split_axis=0...  19.2 us
    all_gather x1, waiting for transfers between devices, on_device(): lax.all_gather(arrived[1], 'tp', axis=2, tiled=True)  15.3 us
    dot_general x1, other arithmetic, span_backward(): jnp.einsum('nts,nsd,ntsd->ntd', grad_scores, key_blk, decays, precision=h...  15.1 us
    all_to_all x1, blocking collectives, on_device(): lax.all_to_all(rows_cot.astype(jnp.bfloat16).reshape(experts, capacity, -...  15.1 us
  transfers between devices with their start and end apart: 7, of which 6 were waited for; matrix products, arithmetic and copies ran while one was open for 28% of the time, Pallas kernels for 0%

commit v1 on v0

--- a/solution.py
+++ b/solution.py
@@ -166,8 +166,16 @@
         * slot_weight[:, None]
     )
     arrived = (
-        lax.all_to_all(
-            rows_in.reshape(experts, capacity, -1), "sp", split_axis=0, concat_axis=1, tiled=True
+        jnp.concatenate(
+            lax.all_to_all(
+                jnp.stack(
+                    jnp.split(rows_in.reshape(experts, capacity, -1), lax.axis_size("sp"), axis=0)
+                ),
+                "sp",
+                0,
+                0,
+            ),
+            axis=1,
         ),
         lax.all_to_all(
             rows_cot.astype(jnp.bfloat16).reshape(experts, capacity, -1),

time: 321 us -> 321 us (level)
  no operation moved by 1% of the time
where the time goes in v1:
time: 321 us; the launch traced here: 320 us
  waiting for transfers between devices  120 us (37%)
  blocking collectives  60.6 us (19%)
  other arithmetic  60 us (19%)
  matrix products  42 us (13%)
  between operations  16.2 us (5%)
  local copies, waits for them, and re-layouts  15.3 us (5%)
  starting transfers between devices  5.89 us (2%)
    reduce_scatter x1, waiting for transfers between devices, on_device(): lax.psum_scatter(lax.dot_general(resid_cols, mixed, (((0,), (0,)), ((), (...  42.4 us
    reduce_scatter x1, waiting for transfers between devices, on_device(): lax.psum_scatter(partial_short, 'tp', scatter_dimension=2, tiled=True)  27.5 us
    all_to_all x1, waiting for transfers between devices, on_device(): lax.all_to_all(summed, 'sp', split_axis=1, concat_axis=0, tiled=True)  21.2 us
    all_gather x1, blocking collectives, entering(): lax.all_gather(a.astype(kind), axis)  19.4 us
    all_to_all x1, blocking collectives, on_device(): lax.all_to_all(jnp.stack(jnp.split(rows_in.reshape(experts, capacity, -1)...  19.2 us
    all_gather x1, waiting for transfers between devices, on_device(): lax.all_gather(arrived[1], 'tp', axis=2, tiled=True)  15.3 us
    dot_general x1, other arithmetic, span_backward(): jnp.einsum('nts,nsd,ntsd->ntd', grad_scores, key_blk, decays, precision=h...  15.1 us
    all_to_all x1, blocking collectives, on_device(): lax.all_to_all(rows_cot.astype(jnp.bfloat16).reshape(experts, capacity, -...  15.1 us
  transfers between devices with their start and end apart: 7, of which 6 were waited for; matrix products, arithmetic and copies ran while one was open for 28% of the time, Pallas kernels for 0%

profile of v1, /device:TPU:0, one launch (start us, length us, event | category | flops | bytes accessed | tf_op | source)
XLA Modules:
  0.0 320.3 jit_solution(5627342192317848681)
XLA Ops:
  11.2 1.2 fusion.27
  12.5 1.1 convert_multiply_fusion
  13.7 1.2 convolution_convert_fusion.4
  15.1 19.2 %all_to_all.26 = bf16[8,1,48,512]{3,2,1,0:T(8,128)(2,1)} all-to-all(bf16[8,1,48,512]{3,2,1,0:T(8,128)(2,1)S(1)} %fusion.44), channel_id=1, replica_groups=mesh['sp'=8,'tp'=4] {'sp'}, dimensions={0} | all-to-all | bytes 786432 | tf_op jit(solution)/shard_map/all_to_all | solution.py:170
  35.1 15.1 %all_to_all.27 = bf16[8,48,512]{2,1,0:T(8,128)(2,1)} all-to-all(bf16[8,48,512]{2,1,0:T(8,128)(2,1)S(1)} %bitcast.261), channel_id=1, replica_groups=mesh['sp'=8,'tp'=4] {'sp'}, dimensions={0} | all-to-all | bytes 786432 | tf_op jit(solution)/shard_map/all_to_all | solution.py:180
  50.2 2.6 all-gather.8.cloned.1.call-done
  52.8 4.0 %fusion.12 = f32[384,512]{1,0:T(8,128)} fusion(bf16[1,2048,512]{2,1,0:T(8,128)(2,1)} %param.27, bf16[1,384,2048]{2,1,0:T(8,128)(2,1)} %all-gather.8.cloned.1.call-done), kind=kOutput, calls=%fused_computation.29 | convolution fusion | flops 805306368 | bytes 4456448 | tf_op jit(solution)/shard_map/erd,edf->erf/dot_general | solution.py:195
  56.8 1.9 fusion.9
  58.7 15.3 %all-gather.10.cloned.1.call-done = bf16[1,384,2048]{2,1,0:T(8,128)(2,1)} async-done(((bf16[1,384,512]{2,1,0:T(8,128)(2,1)}), bf16[1,384,2048]{2,1,0:T(8,128)(2,1)}) %all-gather.10.cloned.1.call-update) | async-done | bytes 1572880 | tf_op jit(solution)/shard_map/all_gather | solution.py:190
  74.0 3.7 %multiply_convert_fusion.1 = (bf16[384,512]{1,0:T(8,128)(2,1)S(1)}, bf16[384,512]{1,0:T(8,128)(2,1)S(1)}) fusion(f32[384,512]{1,0:T(8,128)} %fusion.9, f32[384,512]{1,0:T(8,128)} %fusion.12, bf16[1,512,2048]{2,1,0:T(8,128)(2,1)} %param.28, bf16[1,384,2048]{2,1,0:T(8,128)(2,1)} %all-gather.10.cloned.1.call-done), kind=kOutput, calls=%fused_computation.64 | convolution fusion | flops 807862272 | bytes 6029312 | tf_op jit(solution)/shard_map/erd,efd->erf/dot_general | solution.py:198
  77.8 1.0 fusion.7
  79.6 2.2 fusion.6
  82.4 27.5 %reduce-scatter.3.cloned.1.call-done = bf16[1,384,512]{2,1,0:T(8,128)(2,1)} async-done(((bf16[1,384,2048]{2,1,0:T(8,128)(2,1)}), bf16[1,384,512]{2,1,0:T(8,128)(2,1)}) %reduce-scatter.3.cloned.1.call-update) | async-done | bytes 393232 | tf_op jit(solution)/shard_map/reduce_scatter | solution.py:220
  109.9 1.6 copy.278
  112.0 3.0 reduce.9
  115.1 1.0 reshape.334
  116.1 5.6 %all-to-all-start.2 = ((bf16[8,2,12288]{2,1,0:T(2,128)(2,1)}), bf16[8,2,12288]{2,1,0:T(2,128)(2,1)S(1)}, u32[]{:S(2)}, u32[]{:S(2)}) async-start(bf16[8,2,12288]{2,1,0:T(2,128)(2,1)} %reshape.334), calls=%async_computation.3 | async-start | bytes 786432 | tf_op jit(solution)/shard_map/all_to_all | solution.py:224
  123.5 21.2 %all-to-all-done.2 = bf16[8,2,12288]{2,1,0:T(2,128)(2,1)S(1)} async-done(((bf16[8,2,12288]{2,1,0:T(2,128)(2,1)}), bf16[8,2,12288]{2,1,0:T(2,128)(2,1)S(1)}, u32[]{:S(2)}, u32[]{:S(2)}) %all-to-all-start.2) | async-done | bytes 393248 | tf_op jit(solution)/shard_map/all_to_all | solution.py:224
  145.4 6.9 %all_gather.24 = bf16[128,2048]{1,0:T(8,128)(2,1)S(1)} all-gather(bf16[128,512]{1,0:T(8,128)(2,1)S(1)} %convolution_convert_fusion.6), channel_id=1, replica_groups=mesh['sp'=8,'tp'=4] {'tp'}, dimensions={1}, use_global_device_ids=true | all-gather | bytes 655360 | tf_op jit(solution)/shard_map/all_gather | solution.py:226
  153.4 10.2 %all-gather.12.cloned.1.call-done = bf16[2048,1024]{1,0:T(8,128)(2,1)} async-done(((bf16[256,1024]{1,0:T(8,128)(2,1)}), bf16[2048,1024]{1,0:T(8,128)(2,1)}) %all-gather.12.cloned.1.call-update) | async-done | bytes 4194320 | tf_op jit(solution)/shard_map/all_gather | solution.py:251
  163.5 3.1 convolution_convert_fusion.5
  166.9 1.6 convolution_bitcast_fusion
  168.5 1.1 broadcast.91.clone.1
  169.5 2.1 while.45
  172.5 1.2 reshape.303
  174.4 19.4 %all-gather.2 = bf16[8,4,128]{2,1,0:T(4,128)(2,1)} all-gather(bf16[1,4,128]{2,1,0:T(4,128)(2,1)S(1)} %fusion.55), channel_id=3, replica_groups=mesh['sp'=8,'tp'=4] {'sp'}, dimensions={0}, use_global_device_ids=true | all-gather | bytes 9216 | tf_op jit(solution)/shard_map/all_gather | solution.py:19
  195.9 4.5 %convolution_convert_fusion = bf16[2048,1024]{1,0:T(8,128)(2,1)} fusion(bf16[128,1024]{1,0:T(8,128)(2,1)S(1)} %copy-done.25, bf16[128,2048]{1,0:T(8,128)(2,1)S(1)} %all_gather.24, bf16[128,2048]{1,0:T(8,128)(2,1)} %param.23, f32[128]{0:T(128)} %copy-done.30, f32[2048]{0:T(1024)S(1)} %copy-done.26, f32[128]{0:T(128)} %copy-done.29, ...), kind=kOutput, calls=%fused_computation.15 | convolution fusion | flops 541589504 | bytes 6038528 | tf_op jit(solution)/shard_map/dot_general | solution.py:241
  201.4 9.4 %fusion = (f32[4,2,64,64]{3,2,1,0:T(8,128)}, f32[4,2,64,128,64]{3,4,2,1,0:T(8,128)}) fusion(f32[4,2,128,64]{2,3,1,0:T(8,128)S(1)} %bitcast.245, f32[4,2,128,64]{2,3,1,0:T(8,128)S(1)} %bitcast.257, f32[4,2,64,128]{3,2,1,0:T(8,128)S(1)} %reduce_window_sum.50, pred[64,64]{1,0:T(8,128)(4,1)S(1)} %iota_compare_fusion.2), kind=kLoop, calls=%fused_computation.9 | loop fusion | flops 20938752 | bytes 17698816 | tf_op jit(solution)/shard_map/vmap(ntd,nsd,ntsd->nts)/dot_general | solution.py:81
  211.3 4.5 %fusion.4 = bf16[1,2048,512]{2,1,0:T(8,128)(2,1)} fusion(bf16[384,512]{1,0:T(8,128)(2,1)} %copy-done.21, bf16[1,384,2048]{2,1,0:T(8,128)(2,1)} %all-gather.8.cloned.1.call-done), kind=kOutput, calls=%fused_computation.21 | convolution fusion | flops 806354944 | bytes 4063232 | tf_op jit(solution)/shard_map/erd,erf->edf/dot_general | solution.py:209
  215.9 2.6 fusion.3
  218.6 2.7 fusion.5
  221.6 1.2 fusion.60
  222.9 15.1 %fusion.1 = f32[4,2,64,128]{3,2,1,0:T(8,128)S(1)} fusion(f32[4,2,64,128,64]{3,4,2,1,0:T(8,128)} %get-tuple-element.416, f32[4,2,64,128]{3,2,1,0:T(8,128)S(1)} %bitcast.246, f32[4,2,64,64]{3,2,1,0:T(8,128)S(1)} %copy.217), kind=kLoop, calls=%fused_computation.11 | loop fusion | flops 12517376 | bytes 17432576 | tf_op jit(solution)/shard_map/vmap(nts,nsd,ntsd->ntd)/dot_general | solution.py:84
  238.0 1.4 fusion.26
  239.5 6.3 %multiply_reduce_fusion = f32[4,2,64,128]{3,2,1,0:T(8,128)} fusion(f32[4,2,64,64]{3,2,1,0:T(8,128)S(1)} %fusion.59, f32[4,2,64,128]{3,2,1,0:T(8,128)S(1)} %bitcast.258, f32[4,2,64,128]{3,2,1,0:T(8,128)S(1)} %reduce_window_sum.50, pred[64,64]{1,0:T(8,128)(4,1)S(1)} %iota_compare_fusion.2), kind=kLoop, calls=%fused_computation.12 | loop fusion | flops 20905984 | bytes 921600 | tf_op jit(solution)/shard_map/vmap(nts,ntd,ntsd->nsd)/dot_general | solution.py:88
  245.8 12.8 %while.44 = (s32[]{:T(128)}, f32[4,128,256]{2,1,0:T(8,128)S(1)}, s32[]{:T(128)}, bf16[8,4,128,256]{3,2,1,0:T(8,128)(2,1)}, bf16[8,4,128]{2,1,0:T(4,128)(2,1)}, /*index=5*/s32[]{:T(128)}, s32[]{:T(128)}, s32[]{:T(128)}, s32[]{:T(128)}) while((s32[]{:T(128)}, f32[4,128,256]{2,1,0:T(8,128)S(1)}, s32[]{:T(128)}, ...), condition=%wide.region_17.18_spmd, body=%wide.region_16.17_spmd.sunk | while | flops 393734 | bytes 1315987 | solution.py:34
  246.6 1.1 convert_add_fusion.2
  248.3 1.1 convert_add_fusion.2
  250.1 1.1 convert_add_fusion.2
  252.0 1.1 convert_add_fusion.2
  253.8 1.1 convert_add_fusion.2
  255.5 1.1 convert_add_fusion.2
  257.3 1.1 convert_add_fusion.2
  258.7 2.7 multiply_subtract_fusion
  261.4 1.7 rev.7
  264.7 2.3 fusion.23
  268.4 42.4 %reduce-scatter.5.cloned.1.call-done = bf16[256,1024]{1,0:T(8,128)(2,1)} async-done(((bf16[2048,1024]{1,0:T(8,128)(2,1)}), bf16[256,1024]{1,0:T(8,128)(2,1)}) %reduce-scatter.5.cloned.1.call-update) | async-done | bytes 524304 | tf_op jit(solution)/shard_map/reduce_scatter | solution.py:240
  310.8 2.1 convert_element_type.191
  (172 shorter events, 25.4 us)
Async XLA Ops:
  8.0 48.8 %copy-start = (bf16[1,2048,512]{2,1,0:T(8,128)(2,1)S(1)}, bf16[1,2048,512]{2,1,0:T(8,128)(2,1)}, u32[]{:S(2)}) copy-start(bf16[1,2048,512]{2,1,0:T(8,128)(2,1)} %param.26) | copy-start | bytes 6291460
  8.0 4.5 %copy-start.3 = (bf16[128,2048]{1,0:T(8,128)(2,1)S(1)}, bf16[128,2048]{1,0:T(8,128)(2,1)}, u32[]{:S(2)}) copy-start(bf16[128,2048]{1,0:T(8,128)(2,1)} %param.21) | copy-start | bytes 1572868
  8.0 5.6 %copy-start.26 = (f32[2048]{0:T(1024)S(1)}, f32[2048]{0:T(1024)}, u32[]{:S(2)}) copy-start(f32[2048]{0:T(1024)} %param.22) | copy-start | bytes 24580
  8.0 44.8 %all-gather.8.cloned.1.call-start = ((), (), s32[]{:S(2)}) async-start(), calls=%async_computation.5 | async-start | bytes 1966080 | tf_op jit(solution)/shard_map/all_gather | solution.py:189
  11.2 23.6 %copy-start.19 = (pred[384,128]{1,0:T(8,128)(4,1)}, pred[384,128]{1,0:T(8,128)(4,1)S(1)}, u32[]{:S(2)}) copy-start(pred[384,128]{1,0:T(8,128)(4,1)S(1)} %fusion.34) | copy-start | bytes 147460
  12.5 1.1 copy-start.29
  12.5 21.9 %copy-start.31 = (f32[128,2]{0,1:T(2,128)S(1)}, f32[128,2]{0,1:T(2,128)}, u32[]{:S(2)}) copy-start(f32[128,2]{0,1:T(2,128)} %param.25) | copy-start | bytes 3076
  12.5 22.3 %copy-start.9 = (bf16[128,2048]{1,0:T(8,128)(2,1)S(1)}, bf16[128,2048]{1,0:T(8,128)(2,1)}, u32[]{:S(2)}) copy-start(bf16[128,2048]{1,0:T(8,128)(2,1)} %param.23) | copy-start | bytes 1572868
  34.3 39.7 %all-gather.10.cloned.1.call-start = ((), (), s32[]{:S(2)}) async-start(), calls=%async_computation.6 | async-start | bytes 1966080 | tf_op jit(solution)/shard_map/all_gather | solution.py:190
  50.2 59.7 %reduce-scatter.3.cloned.1.call-start = ((), (), s32[]{:S(2)}) async-start(), calls=%async_computation.7 | async-start | bytes 1966080 | tf_op jit(solution)/shard_map/reduce_scatter | solution.py:220
  52.8 4.0 %copy-start.32 = (bf16[1,384,2048]{2,1,0:T(8,128)(2,1)S(1)}, bf16[1,384,2048]{2,1,0:T(8,128)(2,1)}, u32[]{:S(2)}) copy-start(bf16[1,384,2048]{2,1,0:T(8,128)(2,1)} %all-gather.8.cloned.1.call-done) | copy-start | bytes 4718596
  77.7 1.0 copy-start.22
  77.7 1.0 copy-start.21
  77.7 1.9 copy-start.12
  81.8 81.7 %all-gather.12.cloned.1.call-start = ((), (), s32[]{:S(2)}) async-start(), calls=%async_computation.9 | async-start | bytes 4718592 | tf_op jit(solution)/shard_map/all_gather | solution.py:251
  82.4 39.4 %copy-start.24 = (f32[128,512]{1,0:T(8,128)S(1)}, f32[128,512]{1,0:T(8,128)}, u32[]{:S(2)}) copy-start(f32[128,512]{1,0:T(8,128)} %param.34) | copy-start | bytes 786436
  112.0 10.8 %copy-start.17 = (bf16[128,512]{1,0:T(8,128)(2,1)S(1)}, bf16[128,512]{1,0:T(8,128)(2,1)}, u32[]{:S(2)}) copy-start(bf16[128,512]{1,0:T(8,128)(2,1)} %param.31) | copy-start | bytes 393220
  116.1 29.0 %copy-start.20 = (pred[384,128]{1,0:T(8,128)(4,1)S(1)}, pred[384,128]{1,0:T(8,128)(4,1)}, u32[]{:S(2)}) copy-start(pred[384,128]{1,0:T(8,128)(4,1)} %copy-done.19) | copy-start | bytes 147460
  116.1 28.6 %all-to-all-start.2 = ((bf16[8,2,12288]{2,1,0:T(2,128)(2,1)}), bf16[8,2,12288]{2,1,0:T(2,128)(2,1)S(1)}, u32[]{:S(2)}, u32[]{:S(2)}) async-start(bf16[8,2,12288]{2,1,0:T(2,128)(2,1)} %reshape.334), calls=%async_computation.3 | async-start | bytes 786432 | tf_op jit(solution)/shard_map/all_to_all | solution.py:224
  121.8 124.0 %all-gather.14.cloned.1.call-start = ((), (), s32[]{:S(2)}) async-start(), calls=%async_computation.10 | async-start | bytes 2359296 | tf_op jit(solution)/shard_map/all_gather | solution.py:19
  153.3 13.3 %copy-start.30 = (f32[128]{0:T(128)}, f32[128]{0:T(128)S(1)}, u32[]{:S(2)}) copy-start(f32[128]{0:T(128)S(1)} %broadcast_multiply_fusion) | copy-start | bytes 1540
  171.6 2.1 copy-start.28
  171.7 22.1 %copy-start.16 = (bf16[128,512]{1,0:T(8,128)(2,1)S(1)}, bf16[128,512]{1,0:T(8,128)(2,1)}, u32[]{:S(2)}) copy-start(bf16[128,512]{1,0:T(8,128)(2,1)} %param.32) | copy-start | bytes 393220
  172.4 23.5 %copy-start.25 = (bf16[128,1024]{1,0:T(8,128)(2,1)S(1)}, bf16[128,1024]{1,0:T(8,128)(2,1)}, u32[]{:S(2)}) copy-start(bf16[128,1024]{1,0:T(8,128)(2,1)} %param.30) | copy-start | bytes 786436
  172.4 138.4 %reduce-scatter.5.cloned.1.call-start = ((), (), s32[]{:S(2)}) async-start(), calls=%async_computation.8 | async-start | bytes 4718592 | tf_op jit(solution)/shard_map/reduce_scatter | solution.py:240
  173.7 26.7 %copy-start.5 = (bf16[4,128,256]{2,1,0:T(8,128)(2,1)}, bf16[4,128,256]{2,1,0:T(8,128)(2,1)S(1)}, u32[]{:S(2)}) copy-start(bf16[4,128,256]{2,1,0:T(8,128)(2,1)S(1)} %copy.213) | copy-start | bytes 786436
  200.4 1.0 copy-start.10
  201.3 9.5 %copy-start.2 = (f32[1,4,128,256]{3,2,1,0:T(8,128)S(1)}, f32[1,4,128,256]{3,2,1,0:T(8,128)}, u32[]{:S(2)}) copy-start(f32[1,4,128,256]{3,2,1,0:T(8,128)} %param.35) | copy-start | bytes 1572868
  211.3 4.6 %copy-start.7 = (f32[2,4,128,256]{3,2,1,0:T(8,128)}, f32[2,4,128,256]{3,2,1,0:T(8,128)S(1)}, u32[]{:S(2)}) copy-start(f32[2,4,128,256]{3,2,1,0:T(8,128)S(1)} %get-tuple-element.224) | copy-start | bytes 3145732
  211.3 4.6 %copy-start.23 = (bf16[384,512]{1,0:T(8,128)(2,1)S(1)}, bf16[384,512]{1,0:T(8,128)(2,1)}, u32[]{:S(2)}) copy-start(bf16[384,512]{1,0:T(8,128)(2,1)} %copy-done.22) | copy-start | bytes 1179652
  211.3 4.6 %copy-start.33 = (bf16[1,384,2048]{2,1,0:T(8,128)(2,1)S(1)}, bf16[1,384,2048]{2,1,0:T(8,128)(2,1)}, u32[]{:S(2)}) copy-start(bf16[1,384,2048]{2,1,0:T(8,128)(2,1)} %all-gather.8.cloned.1.call-done) | copy-start | bytes 4718596
  215.9 2.7 copy-start.34
  215.9 2.7 copy-start.35
  215.9 2.7 copy-start.36
  218.6 2.7 copy-start.6
  218.6 3.0 copy-start.13
  222.9 15.1 %copy-start.8 = (f32[2,4,128,256]{3,2,1,0:T(8,128)S(1)}, f32[2,4,128,256]{3,2,1,0:T(8,128)}, u32[]{:S(2)}) copy-start(f32[2,4,128,256]{3,2,1,0:T(8,128)} %copy-done.7) | copy-start | bytes 3145732
  238.0 1.5 copy-start.11
  239.5 19.2 %copy-start.15 = (f32[16,4,8,128]{3,2,1,0:T(8,128)S(1)}, f32[16,4,8,128]{3,2,1,0:T(8,128)}, u32[]{:S(2)}) copy-start(f32[16,4,8,128]{3,2,1,0:T(8,128)} %multiply_bitcast_fusion) | copy-start | bytes 786436
  245.8 12.9 %copy-start.4 = (f32[2,4,128,256]{3,2,1,0:T(8,128)S(1)}, f32[2,4,128,256]{3,2,1,0:T(8,128)}, u32[]{:S(2)}) copy-start(f32[2,4,128,256]{3,2,1,0:T(8,128)} %get-tuple-element.225) | copy-start | bytes 3145732
  245.8 12.9 %copy-start.14 = (f32[16,4,8,128]{3,2,1,0:T(8,128)S(1)}, f32[16,4,8,128]{3,2,1,0:T(8,128)}, u32[]{:S(2)}) copy-start(f32[16,4,8,128]{3,2,1,0:T(8,128)} %convert_bitcast_fusion) | copy-start | bytes 786436
  245.8 12.9 %copy-start.27 = (f32[4,2,128]{2,0,1:T(4,128)S(1)}, f32[4,2,128]{2,0,1:T(4,128)}, u32[]{:S(2)}) copy-start(f32[4,2,128]{2,0,1:T(4,128)} %copy.222) | copy-start | bytes 12292
  263.8 49.1 %copy-start.1 = (bf16[1,2048,512]{2,1,0:T(8,128)(2,1)S(1)}, bf16[1,2048,512]{2,1,0:T(8,128)(2,1)}, u32[]{:S(2)}) copy-start(bf16[1,2048,512]{2,1,0:T(8,128)(2,1)} %param.26) | copy-start | bytes 6291460
  264.7 3.0 copy-start.18
Sparse Core Ops, SparseCore 0:
  34.4 18.3 all-gather.7
  54.4 19.6 all-gather.9
  81.9 27.9 reduce-scatter.2
Sparse Core Ops, SparseCore 1:
  84.4 79.1 all-gather.11
  172.5 47.9 all-gather.13
  224.0 86.8 reduce-scatter.4
